TPU v7x, 32 devices: a whole 2x2x4 slice. The times are simulated.
32 devices in a mesh: sp: 8 (over z, x), tp: 4 (over y, core).
Axes of the slice: x: 2, y: 2, z: 4, core: 2. Of those that a mesh axis runs over, the one named last changes fastest.
Arguments:
- signal: bfloat16 [1024, 1024], P('sp', 'tp'), may hold values from -6 to 6
- step_log: float32 [1024, 64], P('sp', 'tp'), may hold values from -9 to -1.9
- forget_log: float32 [1024, 64], P('sp', 'tp'), may hold values from -1.4 to 0
- damping: float32 [64, 64], P('tp'), may hold values from 0.001 to 1.6
- freq: float32 [64, 64], P('tp'), may hold values from 0 to 50.26544
- in_re: bfloat16 [64, 64, 16], P('tp'), may hold values from -1 to 1
- in_im: bfloat16 [64, 64, 16], P('tp'), may hold values from -1 to 1
- out_re: bfloat16 [64, 16, 64], P('tp'), may hold values from -4 to 4
- out_im: bfloat16 [64, 16, 64], P('tp'), may hold values from -4 to 4
- skip: float32 [1024], P('tp'), may hold values from -4 to 4
- w_out: bfloat16 [1024, 2048], P('tp'), may hold values from -0.1875 to 0.1875
- residual: bfloat16 [1024, 2048], P('sp', 'tp'), may hold values from -60 to 60
- norm_gain: bfloat16 [2048], P('tp'), may hold values from 0.099609375 to 1.8984375
- w_gate: bfloat16 [2048, 5632], P('sp', 'tp'), may hold values from -0.125 to 0.125
- w_up: bfloat16 [2048, 5632], P('sp', 'tp'), may hold values from -0.125 to 0.125
- w_down: bfloat16 [5632, 2048], P('tp', 'sp'), may hold values from -0.078125 to 0.078125
Outputs:
- output: bfloat16 [1024, 2048], P('sp', 'tp')
All inputs are finite; a program needn't handle non-finite values.
Results may differ from a plain program's by a relative error of at most 0.012.
Values may be sent and summed in bfloat16 or wider, within the bound.
A program may use at most 64 MiB of HBM per device.

v0:
```python
import jax
import jax.numpy as jnp
from jax import lax
from jax.sharding import PartitionSpec as P

EPS = 1e-06


def entering(value, axis, join, neutral):
    count, mine = (lax.axis_size(axis), lax.axis_index(axis))
    pieces = jax.tree.map(lambda part: lax.all_gather(part, axis), value)
    subtotal = jax.tree.map(
        lambda part, zero: jnp.full_like(part, 0) + jnp.asarray(zero, part.dtype), value, neutral
    )

    def turn(position, subtotal):
        longer = join(subtotal, jax.tree.map(lambda part: part[position], pieces))
        return jax.tree.map(lambda new, old: jnp.where(position < mine, new, old), longer, subtotal)

    return lax.fori_loop(0, count - 1, turn, subtotal)


def combine(earlier, later):
    first_are, first_aim, first_bre, first_bim = earlier
    second_are, second_aim, second_bre, second_bim = later
    return (
        second_are * first_are - second_aim * first_aim,
        second_are * first_aim + second_aim * first_are,
        second_are * first_bre - second_aim * first_bim + second_bre,
        second_are * first_bim + second_aim * first_bre + second_bim,
    )


def collect(w_gate, w_up, w_down):
    gate_values_wide, up_full = (
        lax.all_gather(w_gate, "sp", axis=0, tiled=True),
        lax.all_gather(w_up, "sp", axis=0, tiled=True),
    )
    down_full = lax.all_gather(w_down, "sp", axis=1, tiled=True)
    return (gate_values_wide, up_full, down_full)


def local_states(elements, length, flat):
    span = 8
    blocks = tuple((item.reshape(length // span, span, flat) for item in elements))

    def advance(carry, block):
        collected = []
        for offset in range(span):
            carry = combine(carry, tuple((member[offset] for member in block)))
            collected.append(carry)
        stacked = tuple((jnp.stack([entry[number] for entry in collected]) for number in range(4)))
        return (carry, stacked)

    unity = jnp.ones((flat,), jnp.float32)
    nothing = jnp.zeros((flat,), jnp.float32)
    finals, stacked = lax.scan(advance, (unity, nothing, nothing, nothing), blocks)
    return (finals, tuple((member.reshape(length, flat) for member in stacked)))


def state_mixer(signal, step_log, forget_log, damping, freq, in_re, in_im, out_re, out_im, skip):
    length = signal.shape[0]
    groups, states = damping.shape
    width = in_re.shape[2]
    step = jnp.exp(step_log)[:, :, None]
    magnitude = jnp.exp(-damping[None] * step)
    angle = freq[None] * step
    decay_re = magnitude * jnp.cos(angle)
    decay_im = magnitude * jnp.sin(angle)
    denom = damping * damping + freq * freq
    factor_re = (-(decay_re - 1.0) * damping + decay_im * freq) / denom
    factor_im = (-decay_im * damping - (decay_re - 1.0) * freq) / denom
    keep = jnp.exp(forget_log)[:, :, None]
    rows = signal.reshape(length, groups, width)
    both_in = jnp.concatenate([in_re, in_im], axis=1)
    driven = jnp.einsum("tgc,gpc->tgp", rows, both_in, preferred_element_type=jnp.float32)
    source_re = driven[:, :, :states]
    source_im = driven[:, :, states:]
    drive_re = factor_re * source_re - factor_im * source_im
    drive_im = factor_re * source_im + factor_im * source_re
    flat = groups * states
    elements = (
        (keep * decay_re).reshape(length, flat),
        (keep * decay_im).reshape(length, flat),
        drive_re.reshape(length, flat),
        drive_im.reshape(length, flat),
    )
    finals, (running_real, cum_im, local_re, local_im) = local_states(elements, length, flat)
    unity = jnp.ones((flat,), jnp.float32)
    nothing = jnp.zeros((flat,), jnp.float32)
    prior = entering(finals, "sp", combine, (unity, nothing, nothing, nothing))
    state_re = local_re + running_real * prior[2][None] - cum_im * prior[3][None]
    state_im = local_im + running_real * prior[3][None] + cum_im * prior[2][None]
    state_readout = jnp.einsum(
        "myq,yzq->myz",
        state_re.reshape(length, groups, states),
        out_re.astype(jnp.float32),
        precision=lax.Precision.HIGHEST,
    ) - jnp.einsum(
        "myq,yzq->myz",
        state_im.reshape(length, groups, states),
        out_im.astype(jnp.float32),
        precision=lax.Precision.HIGHEST,
    )
    value = state_readout.reshape(length, groups * width) + skip * signal.astype(jnp.float32)
    return jax.nn.gelu(value).astype(jnp.bfloat16)


def local(
    signal,
    step_log,
    forget_log,
    damping,
    freq,
    in_re,
    in_im,
    out_re,
    out_im,
    skip,
    w_out,
    residual,
    norm_gain,
    w_gate,
    w_up,
    w_down,
):
    mixed = state_mixer(
        signal, step_log, forget_log, damping, freq, in_re, in_im, out_re, out_im, skip
    )
    partial_value = jnp.dot(mixed, w_out, preferred_element_type=jnp.float32)
    gate_values_wide, up_full, down_full = collect(w_gate, w_up, w_down)
    model_width = w_out.shape[1]
    projected = lax.psum_scatter(
        partial_value.astype(jnp.bfloat16), "tp", scatter_dimension=1, tiled=True
    ).astype(jnp.float32)
    middle = (residual.astype(jnp.float32) + projected).astype(jnp.bfloat16)
    middle_wide = middle.astype(jnp.float32)
    squares = lax.psum(jnp.sum(middle_wide * middle_wide, axis=1), "tp")
    normed = (
        middle_wide
        * lax.rsqrt(squares[:, None] / model_width + EPS)
        * norm_gain.astype(jnp.float32)
    ).astype(jnp.bfloat16)
    piece = lax.all_gather(normed, "tp", axis=1, tiled=True)
    gate = jnp.dot(piece, gate_values_wide, preferred_element_type=jnp.float32)
    up_projected = jnp.dot(piece, up_full, preferred_element_type=jnp.float32)
    hidden = (jax.nn.silu(gate) * up_projected).astype(jnp.bfloat16)
    down_terms = jnp.dot(hidden, down_full, preferred_element_type=jnp.float32)
    down = lax.psum_scatter(
        down_terms.astype(jnp.bfloat16), "tp", scatter_dimension=1, tiled=True
    ).astype(jnp.float32)
    return (middle_wide + 0.5 * down).astype(jnp.bfloat16)


def solution(mesh):
    placed = (
        P("sp", "tp"),
        P("sp", "tp"),
        P("sp", "tp"),
        P("tp", None),
        P("tp", None),
        P("tp", None, None),
        P("tp", None, None),
        P("tp", None, None),
        P("tp", None, None),
        P("tp"),
        P("tp", None),
        P("sp", "tp"),
        P("tp"),
        P("sp", "tp"),
        P("sp", "tp"),
        P("tp", "sp"),
    )
    return jax.shard_map(
        local, mesh=mesh, in_specs=placed, out_specs=P("sp", "tp"), check_vma=False
    )
```

profile of v0, /device:TPU:0, one launch (start us, length us, event | category | flops | bytes accessed | tf_op | source)
XLA Modules:
  0.0 546.8 jit_solution(6999822606888794892)
XLA Ops:
  10.8 1.5 convolution_bitcast_fusion
  12.3 3.4 multiply_add_fusion.9
  20.4 2.1 multiply_multiply_fusion
  22.5 69.1 %while.41 = (s32[]{:T(128)}, f32[1024]{0:T(1024)S(1)}, f32[1024]{0:T(1024)S(1)}, f32[1024]{0:T(1024)S(1)}, f32[1024]{0:T(1024)S(1)}, /*index=5*/f32[16,8,1024]{2...) while((s32[]{:T(128)}, f32[1024]{0:T(1024)S(1)}, ...), condition=%wide.region_1.2_spmd.clone, body=%wide.region_0.1_spmd.clone.sunk | while | flops 118794 | bytes 1156516 | solution.py:57
  22.7 1.3 constant_dynamic-slice_fusion.44
  26.9 1.3 constant_dynamic-slice_fusion.44
  28.2 1.3 constant_dynamic-slice_fusion.42
  31.3 1.3 constant_dynamic-slice_fusion.44
  32.5 1.3 constant_dynamic-slice_fusion.42
  35.6 1.3 constant_dynamic-slice_fusion.44
  36.9 1.3 constant_dynamic-slice_fusion.42
  40.0 1.3 constant_dynamic-slice_fusion.44
  41.2 1.3 constant_dynamic-slice_fusion.42
  45.5 1.3 constant_dynamic-slice_fusion.42
  48.6 1.3 constant_dynamic-slice_fusion.44
  52.9 1.3 constant_dynamic-slice_fusion.44
  54.1 1.3 constant_dynamic-slice_fusion.42
  62.7 1.3 constant_dynamic-slice_fusion.42
  65.8 1.3 constant_dynamic-slice_fusion.44
  67.1 1.3 constant_dynamic-slice_fusion.42
  70.1 1.3 constant_dynamic-slice_fusion.44
  71.4 1.3 constant_dynamic-slice_fusion.42
  74.5 1.3 constant_dynamic-slice_fusion.44
  75.7 1.3 constant_dynamic-slice_fusion.42
  78.8 1.3 constant_dynamic-slice_fusion.44
  80.1 1.3 constant_dynamic-slice_fusion.42
  83.1 1.3 constant_dynamic-slice_fusion.44
  87.4 1.3 constant_dynamic-slice_fusion.44
  88.7 1.3 constant_dynamic-slice_fusion.42
  91.6 32.4 %all-gather = f32[8192]{0:T(1024)S(1)} all-gather(f32[1024]{0:T(1024)S(1)} %get-tuple-element.221), channel_id=2, replica_groups=mesh['sp'=8,'tp'=4] {'sp'}, dimensions={0}, use_global_device_ids=true | all-gather | bytes 36864 | tf_op jit(solution)/shard_map/all_gather | solution.py:11
  124.0 30.6 %all-gather.1 = f32[8192]{0:T(1024)S(1)} all-gather(f32[1024]{0:T(1024)S(1)} %get-tuple-element.222), channel_id=3, replica_groups=mesh['sp'=8,'tp'=4] {'sp'}, dimensions={0}, use_global_device_ids=true | all-gather | bytes 36864 | tf_op jit(solution)/shard_map/all_gather | solution.py:11
  154.7 30.6 %all-gather.2 = f32[8192]{0:T(1024)S(1)} all-gather(f32[1024]{0:T(1024)S(1)} %get-tuple-element.223), channel_id=4, replica_groups=mesh['sp'=8,'tp'=4] {'sp'}, dimensions={0}, use_global_device_ids=true | all-gather | bytes 36864 | tf_op jit(solution)/shard_map/all_gather | solution.py:11
  185.3 30.6 %all-gather.3 = f32[8192]{0:T(1024)S(1)} all-gather(f32[1024]{0:T(1024)S(1)} %get-tuple-element.224), channel_id=5, replica_groups=mesh['sp'=8,'tp'=4] {'sp'}, dimensions={0}, use_global_device_ids=true | all-gather | bytes 36864 | tf_op jit(solution)/shard_map/all_gather | solution.py:11
  216.6 1.3 reshape.136
  218.0 1.3 reshape.137
  219.3 2.3 reshape.138
  221.6 2.3 reshape.139
  224.0 1.9 multiply_add_fusion.8
  231.3 20.9 %reduce-scatter.3.cloned.1.call-done = bf16[128,512]{1,0:T(8,128)(2,1)} async-done(((bf16[128,2048]{1,0:T(8,128)(2,1)}), bf16[128,512]{1,0:T(8,128)(2,1)}) %reduce-scatter.3.cloned.1.call-update) | async-done | bytes 131088 | tf_op jit(solution)/shard_map/reduce_scatter | solution.py:133
  253.2 6.1 %psum.7 = f32[128]{0:T(128)S(1)} all-reduce(f32[128]{0:T(128)S(1)} %fusion.8), channel_id=1, replica_groups=mesh['sp'=8,'tp'=4] {'tp'}, use_global_device_ids=true, to_apply=%region_6.7 | all-reduce | flops 128 | bytes 1024 | tf_op jit(solution)/shard_map/psum | solution.py:138
  260.3 7.1 %all_gather.44 = bf16[128,2048]{1,0:T(8,128)(2,1)S(1)} all-gather(bf16[128,512]{1,0:T(8,128)(2,1)S(1)} %fusion.10), channel_id=1, replica_groups=mesh['sp'=8,'tp'=4] {'tp'}, dimensions={1}, use_global_device_ids=true | all-gather | bytes 655360 | tf_op jit(solution)/shard_map/all_gather | solution.py:144
  267.5 57.7 %all-gather.8.cloned.1.call-done = bf16[2048,1408]{1,0:T(8,128)(2,1)} async-done(((bf16[256,1408]{1,0:T(8,128)(2,1)}), bf16[2048,1408]{1,0:T(8,128)(2,1)}) %all-gather.8.cloned.1.call-update) | async-done | bytes 5767184 | tf_op jit(solution)/shard_map/all_gather | solution.py:36
  325.2 3.6 fusion.35
  328.8 88.7 %all-gather.10.cloned.1.call-done = bf16[2048,1408]{1,0:T(8,128)(2,1)} async-done(((bf16[256,1408]{1,0:T(8,128)(2,1)}), bf16[2048,1408]{1,0:T(8,128)(2,1)}) %all-gather.10.cloned.1.call-update) | async-done | bytes 5767184 | tf_op jit(solution)/shard_map/all_gather | solution.py:37
  417.6 93.0 %all-gather.12.cloned.1.call-done = bf16[1408,2048]{1,0:T(8,128)(2,1)} async-done(((bf16[1408,256]{1,0:T(8,128)(2,1)}), bf16[1408,2048]{1,0:T(8,128)(2,1)}) %all-gather.12.cloned.1.call-update) | async-done | bytes 5767184 | tf_op jit(solution)/shard_map/all_gather | solution.py:39
  510.5 7.1 %convolution_convert_fusion.1 = bf16[128,2048]{1,0:T(8,128)(2,1)} fusion(bf16[1408,2048]{1,0:T(8,128)(2,1)} %all-gather.12.cloned.1.call-done, bf16[128,2048]{1,0:T(8,128)(2,1)S(1)} %all_gather.44, bf16[2048,1408]{1,0:T(8,128)(2,1)} %all-gather.10.cloned.1.call-done, f32[128,1408]{1,0:T(8,128)S(1)} %fusion.35), kind=kOutput, calls=%fused_computation.77 | convolution fusion | flops 1477738496 | bytes 13303808 | tf_op jit(solution)/shard_map/dot_general | solution.py:148
  517.6 20.0 %reduce-scatter.5.cloned.1.call-done = bf16[128,512]{1,0:T(8,128)(2,1)} async-done(((bf16[128,2048]{1,0:T(8,128)(2,1)}), bf16[128,512]{1,0:T(8,128)(2,1)}) %reduce-scatter.5.cloned.1.call-update) | async-done | bytes 131088 | tf_op jit(solution)/shard_map/reduce_scatter | solution.py:149
  537.6 1.6 fusion.11
  (273 shorter events, 53.1 us)
Async XLA Ops:
  7.4 220.9 %copy-start = (bf16[256,2048]{1,0:T(8,128)(2,1)S(1)}, bf16[256,2048]{1,0:T(8,128)(2,1)}, u32[]{:S(2)}) copy-start(bf16[256,2048]{1,0:T(8,128)(2,1)} %param.30) | copy-start | bytes 3145732
  7.4 244.8 %reduce-scatter.3.cloned.1.call-start = ((), (), s32[]{:S(2)}) async-start(), calls=%async_computation.2 | async-start | bytes 655360 | tf_op jit(solution)/shard_map/reduce_scatter | solution.py:133
  12.3 7.3 %copy-start.6 = (f32[128,16]{0,1:T(8,128)S(1)}, f32[128,16]{0,1:T(8,128)}, u32[]{:S(2)}) copy-start(f32[128,16]{0,1:T(8,128)} %param.22) | copy-start | bytes 24580
  217.9 7.9 %copy-start.4 = (bf16[16,16,64]{2,1,0:T(8,128)(2,1)S(1)}, bf16[16,16,64]{2,1,0:T(8,128)(2,1)}, u32[]{:S(2)}) copy-start(bf16[16,16,64]{2,1,0:T(8,128)(2,1)} %param.27) | copy-start | bytes 98308
  218.0 9.0 %copy-start.5 = (bf16[16,16,64]{2,1,0:T(8,128)(2,1)S(1)}, bf16[16,16,64]{2,1,0:T(8,128)(2,1)}, u32[]{:S(2)}) copy-start(bf16[16,16,64]{2,1,0:T(8,128)(2,1)} %param.28) | copy-start | bytes 98308
  221.6 6.7 %copy-start.3 = (bf16[128,256]{1,0:T(8,128)(2,1)S(1)}, bf16[128,256]{1,0:T(8,128)(2,1)}, u32[]{:S(2)}) copy-start(bf16[128,256]{1,0:T(8,128)(2,1)} %param.20) | copy-start | bytes 196612
  221.6 6.7 %copy-start.7 = (f32[256]{0:T(256)S(1)}, f32[256]{0:T(256)}, u32[]{:S(2)}) copy-start(f32[256]{0:T(256)} %param.29) | copy-start | bytes 3076
  223.9 7.3 %copy-start.8 = (bf16[512]{0:T(512)(128)(2,1)S(1)}, bf16[512]{0:T(512)(128)(2,1)}, u32[]{:S(2)}) copy-start(bf16[512]{0:T(512)(128)(2,1)} %param.32) | copy-start | bytes 3076
  224.0 28.3 %copy-start.1 = (bf16[128,512]{1,0:T(8,128)(2,1)S(1)}, bf16[128,512]{1,0:T(8,128)(2,1)}, u32[]{:S(2)}) copy-start(bf16[128,512]{1,0:T(8,128)(2,1)} %param.31) | copy-start | bytes 393220
  229.5 95.7 %all-gather.8.cloned.1.call-start = ((), (), s32[]{:S(2)}) async-start(), calls=%async_computation.3 | async-start | bytes 6488064 | tf_op jit(solution)/shard_map/all_gather | solution.py:36
  230.1 187.5 %all-gather.10.cloned.1.call-start = ((), (), s32[]{:S(2)}) async-start(), calls=%async_computation.4 | async-start | bytes 6488064 | tf_op jit(solution)/shard_map/all_gather | solution.py:37
  230.6 279.9 %all-gather.12.cloned.1.call-start = ((), (), s32[]{:S(2)}) async-start(), calls=%async_computation.5 | async-start | bytes 6488064 | tf_op jit(solution)/shard_map/all_gather | solution.py:39
  231.2 306.4 %reduce-scatter.5.cloned.1.call-start = ((), (), s32[]{:S(2)}) async-start(), calls=%async_computation.6 | async-start | bytes 655360 | tf_op jit(solution)/shard_map/reduce_scatter | solution.py:149
  328.8 208.8 %copy-start.2 = (bf16[128,512]{1,0:T(8,128)(2,1)S(1)}, bf16[128,512]{1,0:T(8,128)(2,1)}, u32[]{:S(2)}) copy-start(bf16[128,512]{1,0:T(8,128)(2,1)} %reduce-scatter.3.cloned.1.call-done) | copy-start | bytes 393220
Sparse Core Ops, SparseCore 0:
  229.6 22.5 reduce-scatter.2
  517.7 19.8 reduce-scatter.4
Sparse Core Ops, SparseCore 1:
  232.1 93.0 all-gather.7
  327.3 90.2 all-gather.9
  419.5 91.0 all-gather.11
where the time goes:
time: 551 us; the launch traced here: 547 us
  waiting for transfers between devices  282 us (51%)
  blocking collectives  137 us (25%)
  local copies, waits for them, and re-layouts  81.1 us (15%)
  matrix products  15.7 us (3%)
  between operations  15.3 us (3%)
  other arithmetic  14.2 us (3%)
    all_gather x4, blocking collectives, entering(): pieces = jax.tree.map(lambda part: lax.all_gather(part, axis), value)  124 us
    all_gather x1, waiting for transfers between devices, collect(): down_full = lax.all_gather(w_down, 'sp', axis=1, tiled=True)  93 us
    all_gather x1, waiting for transfers between devices, collect(): lax.all_gather(w_up, 'sp', axis=0, tiled=True)  88.7 us
    all_gather x1, waiting for transfers between devices, collect(): lax.all_gather(w_gate, 'sp', axis=0, tiled=True)  57.7 us
    slice x64, local copies, waits for them, and re-layouts, advance(): carry = combine(carry, tuple((member[offset] for member in block)))  41.5 us
    reduce_scatter x1, waiting for transfers between devices, local(): lax.psum_scatter(partial_value.astype(jnp.bfloat16), 'tp', scatter_dimens...  20.9 us
    dynamic_update_slice x32, local copies, waits for them, and re-layouts, local_states(): lax.scan(advance, (unity, nothing, nothing, nothing), blocks)  20.5 us
    reduce_scatter x1, waiting for transfers between devices, local(): lax.psum_scatter(down_terms.astype(jnp.bfloat16), 'tp', scatter_dimension...  20 us
  transfers between devices with their start and end apart: 5, of which 5 were waited for; matrix products, arithmetic and copies ran while one was open for 1% of the time, Pallas kernels for 0%

commit v1 on v0

--- a/solution.py
+++ b/solution.py
@@ -1,6 +1,10 @@
+import functools
+
 import jax
 import jax.numpy as jnp
 from jax import lax
+from jax.experimental import pallas as pl
+from jax.experimental.pallas import tpu as pltpu
 from jax.sharding import PartitionSpec as P
 
 EPS = 1e-06
@@ -151,6 +155,426 @@
     ).astype(jnp.float32)
     return (middle_wide + 0.5 * down).astype(jnp.bfloat16)
 
+MESH = pl.DeviceIdType.MESH
+F32 = jnp.float32
+BF16 = jnp.bfloat16
+NT = (((1,), (1,)), ((), ()))
+
+
+def sincos(angle):
+    turns = jnp.floor(angle * 0.6366197723675814 + 0.5)
+    r = angle - turns * 1.5703125
+    r = r - turns * 4.837512969970703125e-4
+    r = r - turns * 7.54978995489188216e-8
+    q = turns.astype(jnp.int32)
+    r2 = r * r
+    s = ((-1.9515295891e-4 * r2 + 8.3321608736e-3) * r2 - 1.6666654611e-1) * r2 * r + r
+    c = (
+        ((2.443315711809948e-5 * r2 - 1.388731625493765e-3) * r2 + 4.166664568298827e-2) * r2 * r2
+        - 0.5 * r2
+        + 1.0
+    )
+    swap = (q & 1) == 1
+    sine = jnp.where(swap, c, s)
+    cosine = jnp.where(swap, s, c)
+    sine = jnp.where((q & 2) == 2, -sine, sine)
+    cosine = jnp.where(((q + 1) & 2) == 2, -cosine, cosine)
+    return sine, cosine
+
+
+def log2(n):
+    return n.bit_length() - 1
+
+
+def fused_kernel(
+    S, T, X, C,
+    signal, step_log, forget_log, damping, freq, b_re, b_im, c_re, c_im, skip, w_out, residual, gain,
+    wg, wu, wd, out,
+    stepx, keepx, dre, dim, lre, lim, rre, rim, fin, finr, part, partr, ssq, ssqr,
+    wgr, wur, wdr, nbuf, mid, pbuf, rc, ry, rx, rz, send_sems, recv_sems,
+):
+    Z, Y = S // X, T // C
+    s, t = lax.axis_index("sp"), lax.axis_index("tp")
+    z, x = lax.div(s, X), lax.rem(s, X)
+    y, c = lax.div(t, C), lax.rem(t, C)
+    rows, chans = signal.shape
+    flat = damping.shape[1]
+    groups = step_log.shape[1]
+    states, width = flat // groups, chans // groups
+    piece, ks = wgr.shape[1:]
+    kt = nbuf.shape[2]
+    model = T * kt
+    count = [0]
+    copies = []
+
+    def send(src, dst, **where):
+        k = count[0]
+        count[0] += 1
+        copy = pltpu.make_async_remote_copy(
+            src_ref=src, dst_ref=dst, send_sem=send_sems.at[k], recv_sem=recv_sems.at[k],
+            device_id=where, device_id_type=MESH,
+        )
+        copy.start()
+        copies.append(copy)
+        return copy
+
+    barrier = pltpu.get_barrier_semaphore()
+    for d in range(1, S):
+        pl.semaphore_signal(barrier, inc=1, device_id={"sp": lax.rem(s + d, S)}, device_id_type=MESH)
+    for d in range(1, T):
+        pl.semaphore_signal(barrier, inc=1, device_id={"tp": lax.rem(t + d, T)}, device_id_type=MESH)
+    pl.semaphore_wait(barrier, S + T - 2)
+
+    def spread(weight, landing):
+        sent = []
+        for d in range(1, S):
+            to = lax.rem(s + d, S)
+            sent.append(send(weight.at[pl.ds(to * piece, piece)], landing.at[s], sp=to))
+        landing[s] = weight[pl.ds(pl.multiple_of(s * piece, 16), piece)]
+        return sent
+
+    gate_copies = spread(wg, wgr)
+
+    lane = lax.broadcasted_iota(jnp.int32, (groups, flat), 1)
+    grow = lax.broadcasted_iota(jnp.int32, (groups, flat), 0)
+    onehot = jnp.where((lane >> log2(states)) == grow, 1.0, 0.0).astype(F32)
+    stepx[...] = jnp.dot(jnp.exp(step_log[...]), onehot, precision=lax.Precision.HIGHEST,
+                         preferred_element_type=F32)
+    keepx[...] = jnp.dot(jnp.exp(forget_log[...]), onehot, precision=lax.Precision.HIGHEST,
+                         preferred_element_type=F32)
+    wide = lax.broadcasted_iota(jnp.int32, (chans, flat), 1) >> log2(states)
+    tall = lax.broadcasted_iota(jnp.int32, (chans, flat), 0) >> log2(width)
+    own = wide == tall
+
+    def block_diagonal(ref):
+        value = ref[...].astype(F32)
+        value = jnp.concatenate([value] * (flat // value.shape[1]), axis=1)
+        return jnp.where(own, value, 0.0).astype(BF16)
+
+    dre[...] = jnp.dot(signal[...], block_diagonal(b_re), preferred_element_type=F32)
+    dim[...] = jnp.dot(signal[...], block_diagonal(b_im), preferred_element_type=F32)
+    denom = damping[...] * damping[...] + freq[...] * freq[...]
+    dn, fn = damping[...] / denom, freq[...] / denom
+    sub = lax.broadcasted_iota(jnp.int32, (8, flat), 0)
+
+    def block(i, carry):
+        at = pl.ds(pl.multiple_of(i * 8, 8), 8)
+        st, kp = stepx[at, :], keepx[at, :]
+        mag = jnp.exp(-damping[...] * st)
+        sine, cosine = sincos(freq[...] * st)
+        zr, zi = mag * cosine, mag * sine
+        fr = zi * fn - (zr - 1.0) * dn
+        fi = -zi * dn - (zr - 1.0) * fn
+        sr, si = dre[at, :], dim[at, :]
+        value = (kp * zr, kp * zi, fr * sr - fi * si, fr * si + fi * sr)
+        for d in (1, 2, 4):
+            ok = sub >= d
+            before = tuple(
+                jnp.where(ok, pltpu.roll(v, d, 0), n) for v, n in zip(value, (1.0, 0.0, 0.0, 0.0))
+            )
+            value = combine(before, value)
+        value = combine(carry, value)
+        rre[at, :], rim[at, :], lre[at, :], lim[at, :] = value
+        return tuple(v[7:8, :] for v in value)
+
+    one, nil = jnp.ones((1, flat), F32), jnp.zeros((1, flat), F32)
+    final = lax.fori_loop(0, rows // 8, block, (one, nil, nil, nil))
+    fold = flat // 128
+    for a in range(4):
+        for k in range(fold):
+            fin[a, k:k + 1, :] = final[a][:, k * 128:(k + 1) * 128]
+    final_copies = []
+    for d in range(1, S):
+        final_copies.append(send(fin, finr.at[s], sp=lax.rem(s + d, S)))
+    up_copies = spread(wu, wur)
+    for copy in final_copies:
+        copy.wait_recv()
+    prior = (jnp.ones((fold, 128), F32),) + (jnp.zeros((fold, 128), F32),) * 3
+    for p in range(S - 1):
+        longer = combine(prior, tuple(finr[p, a] for a in range(4)))
+        prior = tuple(jnp.where(p < s, n, o) for n, o in zip(longer, prior))
+    pre, pim = (
+        jnp.concatenate([v[k:k + 1, :] for k in range(fold)], axis=1) for v in prior[2:]
+    )
+
+    @pl.loop(0, rows // 32)
+    def _(i):
+        at = pl.ds(pl.multiple_of(i * 32, 32), 32)
+        ar, ai = rre[at, :], rim[at, :]
+        lre[at, :] = lre[at, :] + ar * pre - ai * pim
+        lim[at, :] = lim[at, :] + ar * pim + ai * pre
+
+    def readout(state, matrix):
+        high = state.astype(BF16)
+        low = (state - high.astype(F32)).astype(BF16)
+        return lax.dot_general(high, matrix, NT, preferred_element_type=F32) + lax.dot_general(
+            low, matrix, NT, preferred_element_type=F32
+        )
+
+    value = readout(lre[...], block_diagonal(c_re)) - readout(lim[...], block_diagonal(c_im))
+    value = value + skip[...] * signal[...].astype(F32)
+    mixed = jax.nn.gelu(value).astype(BF16)
+
+    part_copies = []
+    for b in range(T):
+        part[b] = jnp.dot(
+            mixed, w_out[:, b * kt:(b + 1) * kt], preferred_element_type=F32
+        ).astype(BF16)
+    for d in range(1, T):
+        to = lax.rem(t + d, T)
+        part_copies.append(send(part.at[to], partr.at[d], tp=to))
+    total = part[t].astype(F32)
+    for d in range(1, T):
+        part_copies[d - 1].wait_recv()
+        total = total + partr[d].astype(F32)
+    middle = (residual[...].astype(F32) + total).astype(BF16)
+    mid[...] = middle
+    wide_mid = middle.astype(F32)
+    ssq[...] = lax.dot_general(
+        jnp.ones((8, kt), F32), wide_mid * wide_mid, NT,
+        precision=lax.Precision.HIGHEST, preferred_element_type=F32,
+    )
+    ssq_copies = [send(ssq, ssqr.at[d], tp=lax.rem(t + d, T)) for d in range(1, T)]
+    squares = ssq[...]
+    for d in range(1, T):
+        ssq_copies[d - 1].wait_recv()
+        squares = squares + ssqr[d]
+    eye = lax.broadcasted_iota(jnp.int32, (rows, rows), 0) == lax.broadcasted_iota(
+        jnp.int32, (rows, rows), 1
+    )
+    squares = jnp.sum(jnp.where(eye, squares[0:1, :], 0.0), axis=1, keepdims=True)
+    normed = mid[...].astype(F32) * lax.rsqrt(squares / model + EPS) * gain[...].astype(F32)
+    here = pl.ds(pl.multiple_of(s * rows, rows), rows)
+    nbuf[t, here, :] = normed.astype(BF16)
+
+    def tokens(zz, xx):
+        return pl.ds(pl.multiple_of((zz * X + xx) * rows, rows), rows)
+
+    def pass_on(block_ref, **where):
+        return send(block_ref, block_ref, **where)
+
+    mine = nbuf.at[t, here]
+    z_copies = [None] + [
+        pass_on(mine, sp=lax.rem(z + d, Z) * X + x) for d in range(1, Z)
+    ]
+    down_copies = spread(wd, wdr)
+    across = [(e, z * X + lax.rem(x + e, X)) for e in range(1, X)]
+    ups = [(e, lax.rem(y + e, Y) * C + c) for e in range(1, Y)]
+    mates = [(e, y * C + lax.rem(c + e, C)) for e in range(1, C)]
+    y_copies, c_copies = [], []
+
+    def to_tp(zz, xx):
+        block_ref = nbuf.at[t, tokens(zz, xx)]
+        for e, to in ups:
+            back = lax.rem(y - e + Y, Y) * C + c
+            y_copies.append((pass_on(block_ref, tp=to), nbuf.at[back, tokens(zz, xx)]))
+        for e, to in mates:
+            c_copies.append(pass_on(block_ref, tp=to))
+
+    done = [0]
+
+    def flush_y(upto):
+        while done[0] < upto:
+            copy, block_ref = y_copies[done[0]]
+            copy.wait_recv()
+            for e, to in mates:
+                c_copies.append(pass_on(block_ref, tp=to))
+            done[0] += 1
+
+    for d in range(Z):
+        zz = lax.rem(z - d + Z, Z)
+        if d:
+            z_copies[d].wait_recv()
+        x_copies = [
+            pass_on(nbuf.at[t, tokens(zz, x)], sp=z * X + lax.rem(x + e, X)) for e in range(1, X)
+        ]
+        to_tp(zz, x)
+        for e in range(1, X):
+            x_copies[e - 1].wait_recv()
+            to_tp(zz, lax.rem(x - e + X, X))
+        flush_y(len(y_copies) - X * (Y - 1))
+    flush_y(len(y_copies))
+    for copy in gate_copies + up_copies + c_copies:
+        copy.wait_recv()
+
+    span = X * rows
+    order = [d for d in range(1, Z)] + [0]
+    first, second, third, fourth = {}, {}, {}, {}
+
+    def at_z(d):
+        return pl.ds(pl.multiple_of(lax.rem(z + d, Z) * span, span), span)
+
+    def stage_hidden(d):
+        at = at_z(d)
+        gate = jnp.zeros((span, piece), F32)
+        up = jnp.zeros((span, piece), F32)
+        for p in range(S):
+            b, o = (p * ks) // kt, (p * ks) % kt
+            left = nbuf[b, at, o:o + ks]
+            gate = gate + lax.dot_general(left, wgr[p], NT, preferred_element_type=F32)
+            up = up + lax.dot_general(left, wur[p], NT, preferred_element_type=F32)
+        return (gate / (1.0 + jnp.exp(-gate)) * up).astype(BF16)
+
+    def stage_core(d, hidden):
+        at = at_z(d)
+        for p in range(S):
+            b, o = (p * ks) // kt, (p * ks) % kt
+            pbuf[b, at, o:o + ks] = jnp.dot(
+                hidden, wdr[p], preferred_element_type=F32
+            ).astype(BF16)
+        first[d] = []
+        for e in range(1, C):
+            for w in range(Y):
+                theirs = w * C + lax.rem(c + e, C)
+                first[d].append(
+                    (w, e, send(pbuf.at[theirs, at], rc.at[d, e - 1, w], tp=y * C + lax.rem(c + e, C)))
+                )
+
+    def stage_y(d):
+        at = at_z(d)
+        for _, _, copy in first[d]:
+            copy.wait_recv()
+        for w in range(Y):
+            acc = pbuf[w * C + c, at, :].astype(F32)
+            for e in range(1, C):
+                acc = acc + rc[d, e - 1, w].astype(F32)
+            pbuf[w * C + c, at, :] = acc.astype(BF16)
+        second[d] = []
+        for e in range(1, Y):
+            to = lax.rem(y + e, Y) * C + c
+            second[d].append(send(pbuf.at[to, at], ry.at[d, e - 1], tp=to))
+
+    def stage_x(d):
+        at = at_z(d)
+        acc = pbuf[t, at, :].astype(F32)
+        for e in range(1, Y):
+            second[d][e - 1].wait_recv()
+            acc = acc + ry[d, e - 1].astype(F32)
+        pbuf[t, at, :] = acc.astype(BF16)
+        third[d] = []
+        for e in range(1, X):
+            to = lax.rem(x + e, X)
+            third[d].append(
+                send(pbuf.at[t, tokens(lax.rem(z + d, Z), to)], rx.at[d, e - 1], sp=z * X + to)
+            )
+
+    def stage_z(d):
+        block_at = tokens(lax.rem(z + d, Z), x)
+        acc = pbuf[t, block_at, :].astype(F32)
+        for e in range(1, X):
+            third[d][e - 1].wait_recv()
+            acc = acc + rx[d, e - 1].astype(F32)
+        if d == 0:
+            return acc
+        pbuf[t, block_at, :] = acc.astype(BF16)
+        fourth[d] = send(pbuf.at[t, block_at], rz.at[d], sp=lax.rem(z + d, Z) * X + x)
+
+    for i, d in enumerate(order):
+        hidden = stage_hidden(d)
+        if i == 0:
+            for copy in down_copies:
+                copy.wait_recv()
+        stage_core(d, hidden)
+        if i:
+            stage_y(order[i - 1])
+    stage_y(order[-1])
+    acc = None
+    for i, d in enumerate(order):
+        stage_x(d)
+        if i:
+            stage_z(order[i - 1])
+    acc = stage_z(0)
+    for d in range(1, Z):
+        fourth[d].wait_recv()
+        acc = acc + rz[d].astype(F32)
+    out[...] = (mid[...].astype(F32) + 0.5 * acc).astype(BF16)
+    for copy in copies:
+        copy.wait_send()
+
+
+def n_copies(S, T, X, C):
+    Z, Y = S // X, T // C
+    gather = (Z - 1) + Z * (X - 1) + S * (Y - 1) + S * (C - 1) + S * (Y - 1) * (C - 1)
+    reduce = Z * (C - 1) * Y + Z * (Y - 1) + Z * (X - 1) + (Z - 1)
+    return 4 * (S - 1) + 2 * (T - 1) + gather + reduce
+
+
+def fused(
+    S, T, signal, step_log, forget_log, damping, freq, in_re, in_im, out_re, out_im, skip, w_out,
+    residual, norm_gain, w_gate, w_up, w_down,
+):
+    X = C = 2
+    Z, Y = S // X, T // C
+    rows, chans = signal.shape
+    groups, states = damping.shape
+    flat = groups * states
+    hidden, ks = w_down.shape
+    piece = hidden // S
+    kt = residual.shape[1]
+    twice = 128 // states
+
+    def pair(a):
+        return jnp.concatenate([a.reshape(chans, states)] * twice, axis=1)
+
+    args = (
+        signal, step_log, forget_log, damping.reshape(1, flat), freq.reshape(1, flat),
+        pair(in_re.transpose(0, 2, 1)), pair(in_im.transpose(0, 2, 1)), pair(out_re), pair(out_im),
+        skip.reshape(1, chans), w_out, residual, norm_gain.reshape(1, kt),
+        w_gate.T, w_up.T, w_down,
+    )
+    n = n_copies(S, T, X, C)
+    big = pltpu.VMEM((rows, flat), F32)
+    landing = pltpu.VMEM((S, piece, ks), BF16)
+    everything = pltpu.VMEM((T, S * rows, kt), BF16)
+    vmem = pl.BlockSpec(memory_space=pltpu.VMEM)
+    return pl.pallas_call(
+        functools.partial(fused_kernel, S, T, X, C),
+        out_shape=jax.ShapeDtypeStruct((rows, kt), BF16),
+        in_specs=[vmem] * len(args),
+        out_specs=vmem,
+        scratch_shapes=[big] * 8 + [
+            pltpu.VMEM((4, flat // 128, 128), F32),
+            pltpu.VMEM((S, 4, flat // 128, 128), F32),
+            pltpu.VMEM((T, rows, kt), BF16),
+            pltpu.VMEM((T, rows, kt), BF16),
+            pltpu.VMEM((8, rows), F32),
+            pltpu.VMEM((T, 8, rows), F32),
+            landing, landing, landing,
+            everything,
+            pltpu.VMEM((rows, kt), BF16),
+            everything,
+            pltpu.VMEM((Z, C - 1, Y, X * rows, kt), BF16),
+            pltpu.VMEM((Z, Y - 1, X * rows, kt), BF16),
+            pltpu.VMEM((Z, X - 1, rows, kt), BF16),
+            pltpu.VMEM((Z, rows, kt), BF16),
+            pltpu.SemaphoreType.DMA((n,)),
+            pltpu.SemaphoreType.DMA((n,)),
+        ],
+        compiler_params=pltpu.CompilerParams(
+            collective_id=0, has_side_effects=True, vmem_limit_bytes=56 * 1024 * 1024
+        ),
+    )(*args)
+
+
+def fits(S, T, signal, damping, residual, w_down):
+    states = damping.shape[1]
+    width = signal.shape[1] // damping.shape[0]
+    hidden, ks = w_down.shape
+    rows, kt = residual.shape
+    powers = all(n & (n - 1) == 0 for n in (states, width))
+    return (
+        S % 2 == 0 and T % 2 == 0 and S * rows * T * kt <= 4 * 1024 * 1024
+        and hidden % S == 0 and (hidden // S) % 16 == 0 and ks % 128 == 0 and kt % ks == 0
+        and rows % 128 == 0 and powers and states <= 128
+        and (damping.size % 1024) == 0
+    )
+
+
+def choose(S, T, *args):
+    if fits(S, T, args[0], args[3], args[11], args[15]):
+        return fused(S, T, *args)
+    return local(*args)
+
 
 def solution(mesh):
     placed = (
@@ -172,5 +596,5 @@
         P("tp", "sp"),
     )
     return jax.shard_map(
-        local, mesh=mesh, in_specs=placed, out_specs=P("sp", "tp"), check_vma=False
-    )
+        functools.partial(choose, mesh.shape["sp"], mesh.shape["tp"]), mesh=mesh, in_specs=placed, out_specs=P("sp", "tp"), check_vma=False
+    )

time: 551 us -> 126 us (0.23)
  waiting for transfers between devices: 282 us -> 0 us
  blocking collectives: 137 us -> 0 us
  Pallas kernels: 0 us -> 114 us
  local copies, waits for them, and re-layouts: 81.1 us -> 9.26 us
  matrix products: 15.7 us -> 0 us
  between operations: 15.3 us -> 0.03 us
  other arithmetic: 14.2 us -> 1.53 us
    all_gather x3 -> x0, waiting for transfers between devices: 239 us -> none  [the longest x1 93 us: collect(): down_full = lax.all_gather(w_down, 'sp', axis=1, tiled=True)]
    all_gather x5 -> x0, blocking collectives: 131 us -> none  [the longest x4 124 us: entering(): pieces = jax.tree.map(lambda part: lax.all_gather(part, axis), value)]
    pallas_call x0 -> x1, Pallas kernels: none -> 114 us  [fused(): pl.pallas_call(functools.partial(fused_kernel, S, T, X, C), out_shape=jax...]
    slice x64 -> x0, local copies, waits for them, and re-layouts: 41.5 us -> none  [advance(): carry = combine(carry, tuple((member[offset] for member in block)))]
    reduce_scatter x2 -> x0, waiting for transfers between devices: 40.9 us -> none  [the longest x1 20.9 us: local(): lax.psum_scatter(partial_value.astype(jnp.bfloat16), 'tp', scatter_dimens...]
    dynamic_update_slice x32 -> x0, local copies, waits for them, and re-layouts: 20.5 us -> none  [local_states(): lax.scan(advance, (unity, nothing, nothing, nothing), blocks)]
    dot_general x6 -> x0, matrix products: 15.7 us -> none  [the longest x1 7.07 us: local(): down_terms = jnp.dot(hidden, down_full, preferred_element_type=jnp.float32)]
    add x51 -> x0, other arithmetic: 8.36 us -> none  [the longest x1 3.41 us: state_mixer(): drive_im = factor_re * source_im + factor_im * source_re]
  transfers between devices with their start and end apart: 5 -> 0, of which waited for: 5 -> 0; matrix products, arithmetic and copies ran while one was open for 1% -> 0% of each run, Pallas kernels for 0% -> 0%
where the time goes in v1:
time: 126 us; the launch traced here: 125 us
  Pallas kernels  114 us (90%)
  local copies, waits for them, and re-layouts  9.26 us (7%)
  other arithmetic  1.53 us (1%)
    pallas_call x1, Pallas kernels, fused(): pl.pallas_call(functools.partial(fused_kernel, S, T, X, C), out_shape=jax...  114 us
    unnamed x25, local copies, waits for them, and re-layouts  7.33 us

profile of v1, /device:TPU:0, one launch (start us, length us, event | category | flops | bytes accessed | tf_op | source)
XLA Modules:
  0.0 124.7 jit_solution(12847780529378246539)
XLA Ops:
  0.0 0.0 copy-start.7
  0.0 0.0 copy-start.9
  0.0 0.0 copy-start.8
  0.0 0.7 copy-done.9
  0.7 0.6 reshape.31.gain
  1.3 0.0 copy-done.7
  1.3 0.7 reshape.24.damping
  2.0 0.0 copy-done.8
  2.0 0.0 copy-start.5
  2.0 0.0 copy-start.6
  2.0 0.7 reshape.25.freq
  2.6 0.0 copy-done.5
  2.7 0.0 copy-start.1
  2.7 0.0 copy-start.2
  2.7 0.7 copy.19.step_log
  3.4 0.0 copy-done.6
  3.4 0.7 copy.20.forget_log
  4.1 0.0 copy-done.1
  4.1 0.0 copy-done.2
  4.1 0.0 copy-start.3
  4.1 0.0 copy-start.4
  4.1 0.8 pad_maximum_fusion
  4.9 0.1 copy-done.3
  5.0 0.0 copy-done.4
  5.0 0.8 pad_maximum_fusion.2
  5.8 0.0 copy-start
  5.8 2.3 %copy.17 = bf16[256,1408]{0,1:T(8,128)(2,1)} copy(bf16[256,1408]{1,0:T(8,128)(2,1)} %param.29) | data formatting | bytes 1441792 | tf_op args[13]
  8.1 0.0 copy-done
  8.1 1.1 copy.18
  9.2 113.9 %shard_map.154 = bf16[128,512]{1,0:T(8,128)(2,1)} custom-call(bf16[128,256]{1,0:T(8,128)(2,1)} %signal.1, f32[128,16]{1,0:T(8,128)} %copy.19.step_log, f32[128,16]{1,0:T(8,128)} %copy.20.forget_log, f32[1,1024]{1,0:T(1,128)} %reshape.24.damping, f32[1,1024]{1,0:T(1,128)} %reshape.25.freq, bf16[256,128]{1,0:T(8,128)(2,1)} %get-tuple-element.5.b_re, ...), custom_call_target="tpu_custom_call" | custom-call | tf_op jit(solution)/shard_map/pallas_call | solution.py:530
  123.1 1.6 %copy.22 = bf16[128,512]{1,0:T(8,128)(2,1)} copy(bf16[128,512]{1,0:T(8,128)(2,1)} %shard_map.154) | data formatting | bytes 262144
Async XLA Ops:
  0.0 1.3 %copy-start.7 = (f32[16,64]{1,0:T(8,128)S(1)}, f32[16,64]{1,0:T(8,128)}, u32[]{:S(2)}) copy-start(f32[16,64]{1,0:T(8,128)} %param.19) | copy-start | bytes 12292
  0.0 0.7 copy-start.9
  0.0 2.0 %copy-start.8 = (f32[16,64]{1,0:T(8,128)S(1)}, f32[16,64]{1,0:T(8,128)}, u32[]{:S(2)}) copy-start(f32[16,64]{1,0:T(8,128)} %param.20) | copy-start | bytes 12292
  2.0 0.7 copy-start.5
  2.0 1.4 %copy-start.6 = (f32[128,16]{0,1:T(8,128)S(1)}, f32[128,16]{0,1:T(8,128)}, u32[]{:S(2)}) copy-start(f32[128,16]{0,1:T(8,128)} %param.18) | copy-start | bytes 24580
  2.7 1.5 %copy-start.1 = (bf16[16,64,16]{1,2,0:T(8,128)(2,1)S(1)}, bf16[16,64,16]{1,2,0:T(8,128)(2,1)}, u32[]{:S(2)}) copy-start(bf16[16,64,16]{1,2,0:T(8,128)(2,1)} %param.21) | copy-start | bytes 98308
  2.7 1.5 %copy-start.2 = (bf16[16,64,16]{1,2,0:T(8,128)(2,1)S(1)}, bf16[16,64,16]{1,2,0:T(8,128)(2,1)}, u32[]{:S(2)}) copy-start(bf16[16,64,16]{1,2,0:T(8,128)(2,1)} %param.22) | copy-start | bytes 98308
  4.1 0.8 copy-start.3
  4.1 0.9 copy-start.4
  5.8 2.3 %copy-start = (bf16[256,1408]{1,0:T(8,128)(2,1)S(1)}, bf16[256,1408]{1,0:T(8,128)(2,1)}, u32[]{:S(2)}) copy-start(bf16[256,1408]{1,0:T(8,128)(2,1)} %param.30) | copy-start | bytes 2162692

commit v2 on v1

--- a/solution.py
+++ b/solution.py
@@ -156,6 +156,7 @@
     return (middle_wide + 0.5 * down).astype(jnp.bfloat16)
 
 MESH = pl.DeviceIdType.MESH
+PUMP = (7, 7, 0, 0, 7, 0)
 F32 = jnp.float32
 BF16 = jnp.bfloat16
 NT = (((1,), (1,)), ((), ()))
@@ -198,9 +199,8 @@
     z, x = lax.div(s, X), lax.rem(s, X)
     y, c = lax.div(t, C), lax.rem(t, C)
     rows, chans = signal.shape
-    flat = damping.shape[1]
-    groups = step_log.shape[1]
-    states, width = flat // groups, chans // groups
+    groups, states = damping.shape
+    flat, width = groups * states, chans // groups
     piece, ks = wgr.shape[1:]
     kt = nbuf.shape[2]
     model = T * kt
@@ -225,23 +225,34 @@
         pl.semaphore_signal(barrier, inc=1, device_id={"tp": lax.rem(t + d, T)}, device_id_type=MESH)
     pl.semaphore_wait(barrier, S + T - 2)
 
-    def spread(weight, landing):
-        sent = []
-        for d in range(1, S):
+    pending = [(w, r, d) for w, r in ((wg, wgr), (wu, wur), (wd, wdr)) for d in range(1, S)]
+    weight_copies = []
+
+    def pump(number):
+        for _ in range(min(number, len(pending))):
+            w, r, d = pending.pop(0)
             to = lax.rem(s + d, S)
-            sent.append(send(weight.at[pl.ds(to * piece, piece)], landing.at[s], sp=to))
-        landing[s] = weight[pl.ds(pl.multiple_of(s * piece, 16), piece)]
-        return sent
-
-    gate_copies = spread(wg, wgr)
+            weight_copies.append(send(w.at[pl.ds(to * piece, piece)], r.at[s], sp=to))
+
+    pump(PUMP[0])
+    for w, r in ((wg, wgr), (wu, wur), (wd, wdr)):
+        r[s] = w[pl.ds(pl.multiple_of(s * piece, 16), piece)]
 
     lane = lax.broadcasted_iota(jnp.int32, (groups, flat), 1)
     grow = lax.broadcasted_iota(jnp.int32, (groups, flat), 0)
     onehot = jnp.where((lane >> log2(states)) == grow, 1.0, 0.0).astype(F32)
-    stepx[...] = jnp.dot(jnp.exp(step_log[...]), onehot, precision=lax.Precision.HIGHEST,
-                         preferred_element_type=F32)
-    keepx[...] = jnp.dot(jnp.exp(forget_log[...]), onehot, precision=lax.Precision.HIGHEST,
-                         preferred_element_type=F32)
+    mine_only = (lane >> log2(states)) == grow
+
+    def flatten(ref):
+        tiled = jnp.concatenate([ref[...]] * groups, axis=1)
+        return jnp.sum(jnp.where(mine_only, tiled, 0.0), axis=0, keepdims=True)
+
+    damp, rate = flatten(damping), flatten(freq)
+    for log_ref, wide_ref in ((step_log, stepx), (forget_log, keepx)):
+        wide_ref[...] = lax.dot_general(
+            jnp.exp(log_ref[...]), onehot, (((0,), (0,)), ((), ())),
+            precision=lax.Precision.HIGHEST, preferred_element_type=F32,
+        )
     wide = lax.broadcasted_iota(jnp.int32, (chans, flat), 1) >> log2(states)
     tall = lax.broadcasted_iota(jnp.int32, (chans, flat), 0) >> log2(width)
     own = wide == tall
@@ -253,15 +264,15 @@
 
     dre[...] = jnp.dot(signal[...], block_diagonal(b_re), preferred_element_type=F32)
     dim[...] = jnp.dot(signal[...], block_diagonal(b_im), preferred_element_type=F32)
-    denom = damping[...] * damping[...] + freq[...] * freq[...]
-    dn, fn = damping[...] / denom, freq[...] / denom
+    denom = damp * damp + rate * rate
+    dn, fn = damp / denom, rate / denom
     sub = lax.broadcasted_iota(jnp.int32, (8, flat), 0)
 
     def block(i, carry):
         at = pl.ds(pl.multiple_of(i * 8, 8), 8)
         st, kp = stepx[at, :], keepx[at, :]
-        mag = jnp.exp(-damping[...] * st)
-        sine, cosine = sincos(freq[...] * st)
+        mag = jnp.exp(-damp * st)
+        sine, cosine = sincos(rate * st)
         zr, zi = mag * cosine, mag * sine
         fr = zi * fn - (zr - 1.0) * dn
         fi = -zi * dn - (zr - 1.0) * fn
@@ -286,7 +297,7 @@
     final_copies = []
     for d in range(1, S):
         final_copies.append(send(fin, finr.at[s], sp=lax.rem(s + d, S)))
-    up_copies = spread(wu, wur)
+    pump(PUMP[1])
     for copy in final_copies:
         copy.wait_recv()
     prior = (jnp.ones((fold, 128), F32),) + (jnp.zeros((fold, 128), F32),) * 3
@@ -323,6 +334,7 @@
     for d in range(1, T):
         to = lax.rem(t + d, T)
         part_copies.append(send(part.at[to], partr.at[d], tp=to))
+    pump(PUMP[2])
     total = part[t].astype(F32)
     for d in range(1, T):
         part_copies[d - 1].wait_recv()
@@ -335,6 +347,7 @@
         precision=lax.Precision.HIGHEST, preferred_element_type=F32,
     )
     ssq_copies = [send(ssq, ssqr.at[d], tp=lax.rem(t + d, T)) for d in range(1, T)]
+    pump(PUMP[3])
     squares = ssq[...]
     for d in range(1, T):
         ssq_copies[d - 1].wait_recv()
@@ -357,49 +370,23 @@
     z_copies = [None] + [
         pass_on(mine, sp=lax.rem(z + d, Z) * X + x) for d in range(1, Z)
     ]
-    down_copies = spread(wd, wdr)
+    pump(PUMP[4])
     across = [(e, z * X + lax.rem(x + e, X)) for e in range(1, X)]
     ups = [(e, lax.rem(y + e, Y) * C + c) for e in range(1, Y)]
     mates = [(e, y * C + lax.rem(c + e, C)) for e in range(1, C)]
-    y_copies, c_copies = [], []
-
-    def to_tp(zz, xx):
+    y_copies, c_copies = [], {d: [] for d in range(Z)}
+
+    def to_tp(chunk, zz, xx):
         block_ref = nbuf.at[t, tokens(zz, xx)]
         for e, to in ups:
             back = lax.rem(y - e + Y, Y) * C + c
-            y_copies.append((pass_on(block_ref, tp=to), nbuf.at[back, tokens(zz, xx)]))
+            y_copies.append((chunk, pass_on(block_ref, tp=to), nbuf.at[back, tokens(zz, xx)]))
         for e, to in mates:
-            c_copies.append(pass_on(block_ref, tp=to))
+            c_copies[chunk].append(pass_on(block_ref, tp=to))
 
     done = [0]
-
-    def flush_y(upto):
-        while done[0] < upto:
-            copy, block_ref = y_copies[done[0]]
-            copy.wait_recv()
-            for e, to in mates:
-                c_copies.append(pass_on(block_ref, tp=to))
-            done[0] += 1
-
-    for d in range(Z):
-        zz = lax.rem(z - d + Z, Z)
-        if d:
-            z_copies[d].wait_recv()
-        x_copies = [
-            pass_on(nbuf.at[t, tokens(zz, x)], sp=z * X + lax.rem(x + e, X)) for e in range(1, X)
-        ]
-        to_tp(zz, x)
-        for e in range(1, X):
-            x_copies[e - 1].wait_recv()
-            to_tp(zz, lax.rem(x - e + X, X))
-        flush_y(len(y_copies) - X * (Y - 1))
-    flush_y(len(y_copies))
-    for copy in gate_copies + up_copies + c_copies:
-        copy.wait_recv()
-
     span = X * rows
-    order = [d for d in range(1, Z)] + [0]
-    first, second, third, fourth = {}, {}, {}, {}
+    hiddens = {}
 
     def at_z(d):
         return pl.ds(pl.multiple_of(lax.rem(z + d, Z) * span, span), span)
@@ -414,6 +401,44 @@
             gate = gate + lax.dot_general(left, wgr[p], NT, preferred_element_type=F32)
             up = up + lax.dot_general(left, wur[p], NT, preferred_element_type=F32)
         return (gate / (1.0 + jnp.exp(-gate)) * up).astype(BF16)
+
+    def compute(chunk):
+        for copy in c_copies[chunk]:
+            copy.wait_recv()
+        if chunk == 0:
+            for copy in weight_copies[:2 * (S - 1)]:
+                copy.wait_recv()
+        hiddens[chunk] = stage_hidden((Z - chunk) % Z)
+
+
+    def flush_y(upto):
+        while done[0] < upto:
+            chunk, copy, block_ref = y_copies[done[0]]
+            copy.wait_recv()
+            for e, to in mates:
+                c_copies[chunk].append(pass_on(block_ref, tp=to))
+            done[0] += 1
+
+    for d in range(Z):
+        zz = lax.rem(z - d + Z, Z)
+        if d:
+            z_copies[d].wait_recv()
+        x_copies = [
+            pass_on(nbuf.at[t, tokens(zz, x)], sp=z * X + lax.rem(x + e, X)) for e in range(1, X)
+        ]
+        to_tp(d, zz, x)
+        for e in range(1, X):
+            x_copies[e - 1].wait_recv()
+            to_tp(d, zz, lax.rem(x - e + X, X))
+        flush_y(len(y_copies) - X * (Y - 1))
+        pump(PUMP[5] if d < Z - 1 else len(pending))
+        if d:
+            compute(d - 1)
+    flush_y(len(y_copies))
+    compute(Z - 1)
+
+    order = [(Z - d) % Z for d in range(Z)]
+    first, second, third, fourth = {}, {}, {}, {}
 
     def stage_core(d, hidden):
         at = at_z(d)
@@ -470,9 +495,9 @@
         fourth[d] = send(pbuf.at[t, block_at], rz.at[d], sp=lax.rem(z + d, Z) * X + x)
 
     for i, d in enumerate(order):
-        hidden = stage_hidden(d)
+        hidden = hiddens[i]
         if i == 0:
-            for copy in down_copies:
+            for copy in weight_copies[2 * (S - 1):]:
                 copy.wait_recv()
         stage_core(d, hidden)
         if i:
@@ -481,8 +506,9 @@
     acc = None
     for i, d in enumerate(order):
         stage_x(d)
-        if i:
+        if i > 1:
             stage_z(order[i - 1])
+    stage_z(order[-1])
     acc = stage_z(0)
     for d in range(1, Z):
         fourth[d].wait_recv()
@@ -517,7 +543,7 @@
         return jnp.concatenate([a.reshape(chans, states)] * twice, axis=1)
 
     args = (
-        signal, step_log, forget_log, damping.reshape(1, flat), freq.reshape(1, flat),
+        signal, step_log.T, forget_log.T, damping, freq,
         pair(in_re.transpose(0, 2, 1)), pair(in_im.transpose(0, 2, 1)), pair(out_re), pair(out_im),
         skip.reshape(1, chans), w_out, residual, norm_gain.reshape(1, kt),
         w_gate.T, w_up.T, w_down,

time: 126 us -> 132 us (1.048)
  Pallas kernels: 114 us -> 123 us
  local copies, waits for them, and re-layouts: 9.26 us -> 6.32 us
    pallas_call x1, Pallas kernels: 114 us -> 123 us  [fused(): pl.pallas_call(functools.partial(fused_kernel, S, T, X, C), out_shape=jax...]
    unnamed x25 -> x11, local copies, waits for them, and re-layouts: 7.33 us -> 5.73 us
    reshape x2 -> x0, local copies, waits for them, and re-layouts: 1.34 us -> none  [the longest x1 0.67 us: fused(): damping.reshape(1, flat)]
where the time goes in v2:
time: 132 us
  Pallas kernels  123 us (93%)
  local copies, waits for them, and re-layouts  6.32 us (5%)
  other arithmetic  2.49 us (2%)
    pallas_call x1, Pallas kernels, fused(): pl.pallas_call(functools.partial(fused_kernel, S, T, X, C), out_shape=jax...  123 us
    unnamed x11, local copies, waits for them, and re-layouts  5.73 us

profile of v2, /device:TPU:0, one launch (start us, length us, event | category | flops | bytes accessed | tf_op | source)
XLA Modules:
  0.0 132.0 jit_solution(15627967927091269241)
XLA Ops:
  0.0 0.0 copy-start.3
  0.0 0.7 copy-done.3
  0.7 0.6 reshape.23.gain
  1.3 0.0 copy-start.1
  1.3 0.0 copy-start.2
  1.3 1.7 %pad_maximum_fusion = (bf16[256,128]{1,0:T(8,128)(2,1)}, bf16[256,128]{1,0:T(8,128)(2,1)}) fusion(bf16[256,64]{1,0:T(8,128)(2,1)} %bitcast.15, bf16[256,64]{1,0:T(8,128)(2,1)} %bitcast.16), kind=kLoop, calls=%fused_computation | loop fusion | flops 262144 | bytes 196608 | tf_op jit(solution)/shard_map/concatenate | solution.py:543
  3.0 0.0 copy-done.1
  3.0 0.0 copy-done.2
  3.0 0.8 pad_maximum_fusion.2
  3.8 0.0 copy-start
  3.8 2.3 %copy.17 = bf16[256,1408]{0,1:T(8,128)(2,1)} copy(bf16[256,1408]{1,0:T(8,128)(2,1)} %param.29) | data formatting | bytes 1441792 | tf_op args[13]
  6.1 0.0 copy-done
  6.1 1.2 copy.18
  7.2 123.1 %shard_map.154 = bf16[128,512]{1,0:T(8,128)(2,1)} custom-call(bf16[128,256]{1,0:T(8,128)(2,1)} %signal.1, f32[16,128]{1,0:T(8,128)} %bitcast.19, f32[16,128]{1,0:T(8,128)} %bitcast.20, f32[16,64]{1,0:T(8,128)} %damping.1, f32[16,64]{1,0:T(8,128)} %freq.1, bf16[256,128]{1,0:T(8,128)(2,1)} %get-tuple-element.5.b_re, bf16[256,128]{1,0:T(8,128)(2,1)} %get-tuple-element.6.b_im, ...), custom_call_target="tpu_custom_call" | custom-call | tf_op jit(solution)/shard_map/pallas_call | solution.py:556
  130.4 1.6 %copy.20 = bf16[128,512]{1,0:T(8,128)(2,1)} copy(bf16[128,512]{1,0:T(8,128)(2,1)} %shard_map.154) | data formatting | bytes 262144
Async XLA Ops:
  0.0 0.7 copy-start.3
  1.3 1.7 %copy-start.1 = (bf16[16,16,64]{2,1,0:T(8,128)(2,1)S(1)}, bf16[16,16,64]{2,1,0:T(8,128)(2,1)}, u32[]{:S(2)}) copy-start(bf16[16,16,64]{2,1,0:T(8,128)(2,1)} %param.23) | copy-start | bytes 98308
  1.3 1.7 %copy-start.2 = (bf16[16,16,64]{2,1,0:T(8,128)(2,1)S(1)}, bf16[16,16,64]{2,1,0:T(8,128)(2,1)}, u32[]{:S(2)}) copy-start(bf16[16,16,64]{2,1,0:T(8,128)(2,1)} %param.24) | copy-start | bytes 98308
  3.8 2.3 %copy-start = (bf16[256,1408]{1,0:T(8,128)(2,1)S(1)}, bf16[256,1408]{1,0:T(8,128)(2,1)}, u32[]{:S(2)}) copy-start(bf16[256,1408]{1,0:T(8,128)(2,1)} %param.30) | copy-start | bytes 2162692
